TPU v7x, 32 devices: a whole 2x2x4 slice. The times are simulated.
32 devices in a mesh: grp: 2 (over x), tp: 16 (over z, y, core).
Axes of the slice: x: 2, y: 2, z: 4, core: 2. Of those that a mesh axis runs over, the one named last changes fastest.
Arguments:
- stream_in: bfloat16 [64, 4, 4096], P('grp'), parts along dimension 0, may hold values from -6 to 6
- state_in: float32 [2, 64, 8, 256, 256], P(None, 'grp', None, 'tp'), parts along dimension 1, may hold values from -0.8 to 0.8
- norm_gain: bfloat16 [2, 4096], replicated, may hold values from 0.099609375 to 1.8984375
- query_weight: bfloat16 [2, 4096, 2048], P(None, None, 'tp'), may hold values from -0.09375 to 0.09375
- key_weight: bfloat16 [2, 4096, 2048], P(None, None, 'tp'), may hold values from -0.09375 to 0.09375
- value_weight: bfloat16 [2, 4096, 8, 256], P(None, None, None, 'tp'), as said below
- gate_weight: bfloat16 [2, 4096, 8, 256], P(None, None, None, 'tp'), may hold values from -0.09375 to 0.09375
- group_gain: bfloat16 [2, 8, 256], P(None, None, 'tp'), may hold values from 0.099609375 to 1.8984375
- output_weight: bfloat16 [2, 8, 256, 4096], P(None, None, 'tp'), may hold values from -0.375 to 0.375
Outputs:
- stream_out: bfloat16 [64, 4, 4096], P('grp', None, 'tp'), parts along dimension 0
- state_out: float32 [2, 64, 8, 256, 256], P(None, 'grp', None, 'tp'), parts along dimension 1
There are 2 independent parts, one for each index of `grp`. A program takes and returns all parts, laid end to end along the dimension named above; an argument that names none is the same for every part. Nothing has to cross between parts.
Inputs may be any that keep to these rules, and one draw needn't show every extreme that they name: `value_weight`: real values; column scales of the value projection differ.
All inputs are finite; a program needn't handle non-finite values.
Results may differ from a plain program's by a relative error of at most 0.024.
Values may be sent and summed in bfloat16 or wider, within the bound.
No kernel may reach another device: no remote copies, remote signals or barrier semaphores. Data moves between devices by JAX's collectives and lax.ppermute only.
A program may use at most 64 MiB of HBM per device.

v0:
```python
import jax
import jax.numpy as jnp
from jax import lax
from jax.sharding import PartitionSpec as P

HEAD_DIM = 256
PAST = 1024
EPS_RMS = 1e-06
EPS_GROUP = 1e-05
ROTARY_BASE = 10000.0


def log_decays(count):
    return jnp.log(1.0 - jnp.power(2.0, -5.0 - jnp.arange(count, dtype=jnp.float32)))


def decay_tables(log_gamma, count):
    steps = jnp.arange(count, dtype=jnp.float32)
    gap = steps[:, None] - steps[None, :]
    intra = jnp.where(
        gap[None] >= 0, jnp.exp(log_gamma[:, None, None] * jnp.maximum(gap, 0.0)[None]), 0.0
    )
    q_decay = jnp.exp(log_gamma[None, :] * (steps[:, None] + 1.0))
    k_decay = jnp.exp(log_gamma[None, :] * (count - 1.0 - steps[:, None]))
    block_decay = jnp.exp(log_gamma * count)
    return (intra, q_decay, k_decay, block_decay)


def rotate(values, offset):
    half_dim = values.shape[-1] // 2
    freqs = jnp.power(
        ROTARY_BASE, -jnp.arange(half_dim, dtype=jnp.float32) * (2.0 / values.shape[-1])
    )
    places = (offset + jnp.arange(values.shape[1])).astype(jnp.float32)
    angles = places[:, None] * freqs[None, :]
    cosine = jnp.cos(angles)[None, :, None, :]
    sine = jnp.sin(angles)[None, :, None, :]
    first = values[..., :half_dim]
    second = values[..., half_dim:]
    return jnp.concatenate(
        [first * cosine - second * sine, second * cosine + first * sine], axis=-1
    )


def local(
    stream_in,
    state_in,
    norm_gain,
    query_weight,
    key_weight,
    value_weight,
    gate_weight,
    group_gain,
    output_weight,
):
    seqs, new_tok, width = stream_in.shape
    heads, local_dim = (value_weight.shape[2], value_weight.shape[3])
    head_dim = HEAD_DIM
    log_gamma = log_decays(heads)
    intra, q_decay, k_decay, block_decay = decay_tables(log_gamma, new_tok)
    highest = lax.Precision.HIGHEST
    share_cols = width // lax.axis_size("tp")
    col_start = lax.axis_index("tp") * share_cols
    layers = state_in.shape[0]
    stream = stream_in
    stream_share = stream_in
    new_states = []
    for layer_no in range(layers):
        stream_f = stream.astype(jnp.float32)
        normed = stream_f * lax.rsqrt(
            jnp.mean(stream_f * stream_f, axis=-1, keepdims=True) + EPS_RMS
        )
        normed = (normed * norm_gain[layer_no].astype(jnp.float32)).astype(jnp.bfloat16)
        flat = normed.reshape(seqs * new_tok, width)
        query_part = jnp.dot(flat, query_weight[layer_no], preferred_element_type=jnp.float32)
        query_part = query_part.astype(jnp.bfloat16).reshape(seqs, new_tok, -1)
        key_part = jnp.dot(flat, key_weight[layer_no], preferred_element_type=jnp.float32)
        key_part = key_part.astype(jnp.bfloat16).reshape(seqs, new_tok, -1)

        def project_local(weight):
            result = jnp.dot(
                flat, weight.reshape(width, heads * local_dim), preferred_element_type=jnp.float32
            )
            result = lax.optimization_barrier(result.astype(jnp.bfloat16))
            return result.astype(jnp.float32).reshape(seqs, new_tok, heads, local_dim)

        values_f = project_local(value_weight[layer_no])
        gates_f = project_local(gate_weight[layer_no])
        queries, key_rows = (
            lax.all_gather(query_part, "tp", axis=2, tiled=True),
            lax.all_gather(key_part, "tp", axis=2, tiled=True),
        )
        queries = queries.astype(jnp.float32).reshape(seqs, new_tok, heads, head_dim)
        key_rows = key_rows.astype(jnp.float32).reshape(seqs, new_tok, heads, head_dim)
        rot_q = rotate(queries, PAST)
        rot_k = rotate(key_rows, PAST) * head_dim ** (-0.5)
        scores = jnp.einsum("bthd,bshd->bhts", rot_q, rot_k, precision=highest) * intra[None]
        inner = jnp.einsum("bhts,bshe->bthe", scores, values_f, precision=highest)
        state = state_in[layer_no]
        carried = (
            jnp.einsum("bthd,bhed->bthe", rot_q, state, precision=highest)
            * q_decay[None, :, :, None]
        )
        mixed = inner + carried
        new_state = state * block_decay[None, :, None, None] + jnp.einsum(
            "bthe,bthd->bhed", values_f, rot_k * k_decay[None, :, :, None], precision=highest
        )
        new_states.append(new_state)
        totals, squares = lax.psum((jnp.sum(mixed, axis=-1), jnp.sum(mixed * mixed, axis=-1)), "tp")
        mean_o = (totals / head_dim)[..., None]
        var_o = (squares / head_dim)[..., None] - mean_o * mean_o
        normal = (
            (mixed - mean_o)
            * lax.rsqrt(var_o + EPS_GROUP)
            * group_gain[layer_no].astype(jnp.float32)[None, None]
        )
        gated = (jax.nn.silu(gates_f) * normal).astype(jnp.bfloat16)
        partial_out = jnp.dot(
            gated.reshape(seqs * new_tok, heads * local_dim),
            output_weight[layer_no].reshape(heads * local_dim, width),
            preferred_element_type=jnp.float32,
        ).reshape(seqs, new_tok, width)
        share_out = lax.psum_scatter(partial_out, "tp", scatter_dimension=2, tiled=True)
        own_cols = lax.dynamic_slice_in_dim(stream, col_start, share_cols, 2)
        stream_share = (own_cols.astype(jnp.float32) + share_out).astype(jnp.bfloat16)
        if layer_no + 1 < layers:
            stream = lax.all_gather(stream_share, "tp", axis=2, tiled=True)
    result = stream_share
    return (result, jnp.stack(new_states))


def solution(mesh):
    in_specs = (
        P("grp", None, None),
        P(None, "grp", None, "tp", None),
        P(),
        P(None, None, "tp"),
        P(None, None, "tp"),
        P(None, None, None, "tp"),
        P(None, None, None, "tp"),
        P(None, None, "tp"),
        P(None, None, "tp", None),
    )
    out_specs = (P("grp", None, "tp"), P(None, "grp", None, "tp", None))
    return jax.shard_map(local, mesh=mesh, in_specs=in_specs, out_specs=out_specs, check_vma=False)
```

profile of v0, /device:TPU:0, one launch (start us, length us, event | category | flops | bytes accessed | tf_op | source)
XLA Modules:
  0.0 433.5 jit_solution(2907268632619906550)
XLA Ops:
  7.3 0.7 bitcast_convert_fusion
  8.0 1.8 fusion.10
  9.9 0.8 slice_convert_fusion
  10.7 1.9 fusion.12
  12.6 0.3 reshape.316
  12.9 1.8 convolution_convert_fusion.4
  14.8 0.4 convolution_convert_fusion.5
  15.2 24.6 %all_gather.15 = bf16[32,4,2048]{2,1,0:T(4,128)(2,1)S(1)} all-gather(bf16[32,4,128]{2,1,0:T(4,128)(2,1)S(1)} %bitcast.115), channel_id=1, replica_groups=mesh['grp'=2,'tp'=16] {'tp'}, dimensions={2}, use_global_device_ids=true | all-gather | bytes 557056 | tf_op jit(solution)/shard_map/all_gather | solution.py:90
  39.8 19.0 %all_gather.16 = bf16[32,4,2048]{2,1,0:T(4,128)(2,1)S(1)} all-gather(bf16[32,4,128]{2,1,0:T(4,128)(2,1)S(1)} %bitcast.114), channel_id=1, replica_groups=mesh['grp'=2,'tp'=16] {'tp'}, dimensions={2}, use_global_device_ids=true | all-gather | bytes 557056 | tf_op jit(solution)/shard_map/all_gather | solution.py:91
  58.9 0.1 convert.11
  59.0 0.1 convert.10
  59.3 0.6 multiply_subtract_fusion.2
  59.9 6.9 %fusion.4 = f32[32,8,4,16]{3,2,1,0:T(4,128)} fusion(f32[2,32,8,16,256]{4,3,2,1,0:T(8,128)} %param.10, f32[32,4,8,128]{3,1,2,0:T(4,128)S(1)} %get-tuple-element.46, f32[32,4,8,128]{3,1,2,0:T(4,128)S(1)} %get-tuple-element.47), kind=kOutput, calls=%fused_computation.7 | convolution fusion | flops 50593792 | bytes 5308416 | tf_op jit(solution)/shard_map/bthd,bhed->bthe/dot_general | solution.py:101
  66.8 2.0 copy.76
  68.9 2.7 fusion.56
  71.5 0.4 convolution_convert_fusion.6
  72.0 0.2 reshape.319
  72.3 2.3 convolution_multiply_fusion.1
  74.6 1.0 fusion.38
  75.6 0.3 copy.75
  75.9 2.7 fusion.55
  78.7 0.4 convolution_convert_fusion.7
  79.1 0.2 reshape.338
  79.3 0.3 copy.73
  79.6 1.8 fusion.54
  81.4 0.2 fusion.51
  81.6 59.1 %all-reduce.1 = (f32[32,4,8]{0,2,1:T(8,128)S(1)}, f32[32,4,8]{0,2,1:T(8,128)S(1)}) all-reduce(f32[32,4,8]{0,2,1:T(8,128)S(1)} %get-tuple-element.15, f32[32,4,8]{0,2,1:T(8,128)S(1)} %get-tuple-element.14), channel_id=1, replica_groups=mesh['grp'=2,'tp'=16] {'tp'}, use_global_device_ids=true, to_apply=%region_4.5 | all-reduce | flops 2048 | bytes 16384 | tf_op jit(solution)/shard_map/psum | solution.py:109
  140.9 1.8 fusion.57
  142.8 0.9 constant_dynamic-slice_fusion
  143.6 58.3 %reduce-scatter.3.cloned.1.call-done = f32[32,4,256]{2,0,1:T(8,128)} async-done(((f32[32,4,4096]{2,0,1:T(8,128)}), f32[32,4,256]{2,0,1:T(8,128)}) %reduce-scatter.3.cloned.1.call-update) | async-done | bytes 131088 | tf_op jit(solution)/shard_map/reduce_scatter | solution.py:123
  201.9 1.5 add_convert_fusion.1
  203.5 0.3 reduce-scatter.5.cloned.1.call-start
  203.8 36.5 %all-gather.2.cloned.1.call-done = bf16[32,4,4096]{2,0,1:T(8,128)(2,1)} async-done(((bf16[32,4,256]{2,0,1:T(8,128)(2,1)}), bf16[32,4,4096]{2,0,1:T(8,128)(2,1)}) %all-gather.2.cloned.1.call-update) | async-done | bytes 1048592 | tf_op jit(solution)/shard_map/all_gather | solution.py:127
  240.3 1.5 fusion.13
  241.8 1.5 fusion.15
  243.4 0.8 copy.78
  244.2 0.3 reshape.326
  244.5 1.7 convolution_convert_fusion
  246.2 1.7 convolution_convert_fusion.1
  248.0 0.4 convolution_convert_fusion.2
  248.4 0.4 convolution_convert_fusion.3
  248.9 0.2 reshape.329
  249.1 21.5 %all_gather.19 = bf16[32,4,2048]{2,1,0:T(4,128)(2,1)S(1)} all-gather(bf16[32,4,128]{2,1,0:T(4,128)(2,1)S(1)} %bitcast.113), channel_id=1, replica_groups=mesh['grp'=2,'tp'=16] {'tp'}, dimensions={2}, use_global_device_ids=true | all-gather | bytes 557056 | tf_op jit(solution)/shard_map/all_gather | solution.py:91
  270.6 18.9 %all_gather.18 = bf16[32,4,2048]{2,1,0:T(4,128)(2,1)S(1)} all-gather(bf16[32,4,128]{2,1,0:T(4,128)(2,1)S(1)} %bitcast.112), channel_id=1, replica_groups=mesh['grp'=2,'tp'=16] {'tp'}, dimensions={2}, use_global_device_ids=true | all-gather | bytes 557056 | tf_op jit(solution)/shard_map/all_gather | solution.py:90
  289.5 0.2 reshape.346
  289.6 1.0 copy.80
  290.7 0.1 convert.12
  290.8 0.1 convert.13
  291.0 0.5 multiply_subtract_fusion
  291.4 0.8 copy-done.8
  292.2 6.6 %fusion = f32[32,8,4,16]{3,2,1,0:T(4,128)} fusion(f32[2,32,8,16,256]{4,3,2,1,0:T(8,128)} %param.10, f32[32,4,8,128]{3,1,2,0:T(4,128)S(1)} %get-tuple-element.44, f32[32,4,8,128]{3,1,2,0:T(4,128)S(1)} %get-tuple-element.45), kind=kOutput, calls=%fused_computation.2 | convolution fusion | flops 50593792 | bytes 5308416 | tf_op jit(solution)/shard_map/bthd,bhed->bthe/dot_general | solution.py:101
  298.8 1.3 copy.83
  300.1 3.4 convolution_multiply_fusion
  303.5 1.0 fusion.35
  304.5 0.3 copy.82
  304.8 0.2 fusion.50
  305.0 59.2 %all-reduce = (f32[32,4,8]{0,2,1:T(8,128)S(1)}, f32[32,4,8]{0,2,1:T(8,128)S(1)}) all-reduce(f32[32,4,8]{0,2,1:T(8,128)S(1)} %get-tuple-element.13, f32[32,4,8]{0,2,1:T(8,128)S(1)} %get-tuple-element.12), channel_id=1, replica_groups=mesh['grp'=2,'tp'=16] {'tp'}, use_global_device_ids=true, to_apply=%region_10.11 | all-reduce | flops 2048 | bytes 16384 | tf_op jit(solution)/shard_map/psum | solution.py:109
  364.4 1.8 fusion.58
  366.3 4.5 %fusion.7 = f32[1,32,8,16,256]{4,3,2,1,0:T(8,128)S(1)} fusion(f32[2,32,8,16,256]{4,3,2,1,0:T(8,128)} %param.10, f32[8]{0:T(128)S(1)} %multiply_exponential_fusion.1, f32[32,4,8,128]{3,1,2,0:T(4,128)S(1)} %copy-done.5, f32[32,4,8,128]{3,1,2,0:T(4,128)S(1)} %copy-done.3, f32[4,8]{0,1:T(8,128)S(1)} %copy.85, bf16[32,4,8,16]{3,2,1,0:T(8,128)(2,1)S(1)} %reshape.319), kind=kOutput, calls=%fused_computation.10 | convolution fusion | flops 52953088 | bytes 9470112 | tf_op jit(solution)/shard_map/bthe,bthd->bhed/dot_general | solution.py:105
  370.8 4.5 %fusion.3 = f32[1,32,8,16,256]{4,3,2,1,0:T(8,128)S(1)} fusion(f32[2,32,8,16,256]{4,3,2,1,0:T(8,128)} %param.10, f32[8]{0:T(128)S(1)} %multiply_exponential_fusion.1, f32[32,4,8,128]{3,1,2,0:T(4,128)S(1)} %copy-done.7, f32[32,4,8,128]{3,1,2,0:T(4,128)S(1)} %get-tuple-element.28, f32[4,8]{0,1:T(8,128)S(1)} %copy.85, bf16[32,4,8,16]{3,2,1,0:T(8,128)(2,1)S(1)} %reshape.329), kind=kOutput, calls=%fused_computation.5 | convolution fusion | flops 52953088 | bytes 9470112 | tf_op jit(solution)/shard_map/bthe,bthd->bhed/dot_general | solution.py:105
  375.3 4.4 %pad_maximum_fusion = f32[2,32,8,16,256]{4,3,2,1,0:T(8,128)} fusion(f32[1,32,8,16,256]{4,3,2,1,0:T(8,128)S(1)} %fusion.3, f32[1,32,8,16,256]{4,3,2,1,0:T(8,128)S(1)} %fusion.7), kind=kLoop, calls=%fused_computation | loop fusion | flops 2097152 | bytes 16777216 | tf_op jit(solution)/shard_map/stack | solution.py:129
  379.8 45.6 %reduce-scatter.5.cloned.1.call-done = f32[32,4,256]{2,0,1:T(8,128)} async-done(((f32[32,4,4096]{2,0,1:T(8,128)}), f32[32,4,256]{2,0,1:T(8,128)}) %reduce-scatter.5.cloned.1.call-update) | async-done | bytes 131088 | tf_op jit(solution)/shard_map/reduce_scatter | solution.py:123
  425.4 0.9 add_convert_fusion
  426.3 0.7 copy.88
  (45 shorter events, 1.0 us)
Async XLA Ops:
  7.2 194.8 %reduce-scatter.3.cloned.1.call-start = ((), (), s32[]{:S(2)}) async-start(), calls=%async_computation.2 | async-start | bytes 2228224 | tf_op jit(solution)/shard_map/reduce_scatter | solution.py:123
  12.9 1.9 copy-start.11
  59.9 12.4 %copy-start.2 = (f32[32,4,8,128]{3,1,2,0:T(4,128)}, f32[32,4,8,128]{3,1,2,0:T(4,128)S(1)}, u32[]{:S(2)}) copy-start(f32[32,4,8,128]{3,1,2,0:T(4,128)S(1)} %get-tuple-element.32) | copy-start | bytes 1572868
  59.9 12.4 %copy-start.4 = (f32[32,4,8,128]{3,1,2,0:T(4,128)}, f32[32,4,8,128]{3,1,2,0:T(4,128)S(1)}, u32[]{:S(2)}) copy-start(f32[32,4,8,128]{3,1,2,0:T(4,128)S(1)} %get-tuple-element.33) | copy-start | bytes 1572868
  79.6 1.9 copy-start.9
  142.7 97.6 %all-gather.2.cloned.1.call-start = ((), (), s32[]{:S(2)}) async-start(), calls=%async_computation.3 | async-start | bytes 1114112 | tf_op jit(solution)/shard_map/all_gather | solution.py:127
  203.5 221.9 %reduce-scatter.5.cloned.1.call-start = ((), (), s32[]{:S(2)}) async-start(), calls=%async_computation.4 | async-start | bytes 2228224 | tf_op jit(solution)/shard_map/reduce_scatter | solution.py:123
  244.5 3.5 copy-start
  246.2 2.2 copy-start.1
  291.4 0.8 copy-start.8
  291.4 8.7 %copy-start.6 = (f32[32,4,8,128]{3,1,2,0:T(4,128)}, f32[32,4,8,128]{3,1,2,0:T(4,128)S(1)}, u32[]{:S(2)}) copy-start(f32[32,4,8,128]{3,1,2,0:T(4,128)S(1)} %get-tuple-element.29) | copy-start | bytes 1572868
  303.5 60.8 %copy-start.10 = (f32[32,4,8,16]{0,3,2,1:T(8,128)S(1)}, f32[32,4,8,16]{0,3,2,1:T(8,128)}, u32[]{:S(2)}) copy-start(f32[32,4,8,16]{0,3,2,1:T(8,128)} %copy.80) | copy-start | bytes 196612
  364.4 2.0 copy-start.3
  364.4 1.9 copy-start.5
  366.3 4.5 %copy-start.7 = (f32[32,4,8,128]{3,1,2,0:T(4,128)S(1)}, f32[32,4,8,128]{3,1,2,0:T(4,128)}, u32[]{:S(2)}) copy-start(f32[32,4,8,128]{3,1,2,0:T(4,128)} %copy-done.6) | copy-start | bytes 1572868
Sparse Core Ops, SparseCore 0:
  142.8 59.0 reduce-scatter.2
  204.7 35.5 all-gather.1
  366.3 58.9 reduce-scatter.4
where the time goes:
time: 434 us
  blocking collectives  202 us (47%)
  waiting for transfers between devices  140 us (32%)
  matrix products  41.1 us (9%)
  other arithmetic  17.9 us (4%)
  local copies, waits for them, and re-layouts  17.2 us (4%)
  between operations  14.2 us (3%)
    psum x2, blocking collectives, local(): lax.psum((jnp.sum(mixed, axis=-1), jnp.sum(mixed * mixed, axis=-1)), 'tp')  118 us
    reduce_scatter x2, waiting for transfers between devices, local(): lax.psum_scatter(partial_out, 'tp', scatter_dimension=2, tiled=True)  104 us
    all_gather x2, blocking collectives, local(): lax.all_gather(query_part, 'tp', axis=2, tiled=True)  43.5 us
    all_gather x2, blocking collectives, local(): lax.all_gather(key_part, 'tp', axis=2, tiled=True)  40.6 us
    all_gather x1, waiting for transfers between devices, local(): stream = lax.all_gather(stream_share, 'tp', axis=2, tiled=True)  36.5 us
    dot_general x2, matrix products, local(): jnp.einsum('bthd,bhed->bthe', rot_q, state, precision=highest)  13.5 us
    dot_general x2, matrix products, local(): jnp.einsum('bthe,bthd->bhed', values_f, rot_k * k_decay[None, :, :, None]...  8.98 us
  transfers between devices with their start and end apart: 3, of which 3 were waited for; matrix products, arithmetic and copies ran while one was open for 3% of the time, Pallas kernels for 0%

commit v1 on v0

--- a/solution.py
+++ b/solution.py
@@ -8,6 +8,22 @@
 EPS_RMS = 1e-06
 EPS_GROUP = 1e-05
 ROTARY_BASE = 10000.0
+
+
+def collect(x, axis, dim):
+    ways, here, lap = (lax.axis_size(axis), lax.axis_index(axis), x.shape[dim])
+    dims = [n * ways if d == dim else n for d, n in enumerate(x.shape)]
+    full = lax.dynamic_update_slice_in_dim(jnp.zeros(dims, x.dtype), x, here * lap, axis=dim)
+    going_up = going_down = x
+    for far in range(1, ways // 2 + 1):
+        going_up = lax.ppermute(going_up, axis, [(d, (d + 1) % ways) for d in range(ways)])
+        full = lax.dynamic_update_slice_in_dim(full, going_up, (here - far) % ways * lap, axis=dim)
+        if 2 * far < ways:
+            going_down = lax.ppermute(going_down, axis, [(d, (d - 1) % ways) for d in range(ways)])
+            full = lax.dynamic_update_slice_in_dim(
+                full, going_down, (here + far) % ways * lap, axis=dim
+            )
+    return full
 
 
 def log_decays(count):
@@ -124,7 +140,7 @@
         own_cols = lax.dynamic_slice_in_dim(stream, col_start, share_cols, 2)
         stream_share = (own_cols.astype(jnp.float32) + share_out).astype(jnp.bfloat16)
         if layer_no + 1 < layers:
-            stream = lax.all_gather(stream_share, "tp", axis=2, tiled=True)
+            stream = collect(stream_share, "tp", 2)
     result = stream_share
     return (result, jnp.stack(new_states))
 

time: 434 us -> 455 us (1.048)
  starting transfers between devices: 0.34 us -> 31.4 us
  waiting for transfers between devices: 140 us -> 123 us
  local copies, waits for them, and re-layouts: 17.2 us -> 23.2 us
    all_gather x1 -> x0, waiting for transfers between devices: 36.5 us -> none  [local(): stream = lax.all_gather(stream_share, 'tp', axis=2, tiled=True)]
    ppermute x0 -> x15, starting transfers between devices: none -> 31.3 us  [the longest x7 31.3 us: collect(): lax.ppermute(going_down, axis, [(d, (d - 1) % ways) for d in range(ways)])]
    ppermute x0 -> x15, waiting for transfers between devices: none -> 19.7 us  [the longest x8 19.6 us: collect(): lax.ppermute(going_up, axis, [(d, (d + 1) % ways) for d in range(ways)])]
  transfers between devices with their start and end apart: 3 -> 17, of which waited for: 3 -> 10; matrix products, arithmetic and copies ran while one was open for 3% -> 3% of each run, Pallas kernels for 0% -> 0%
where the time goes in v1:
time: 455 us; the launch traced here: 454 us
  blocking collectives  202 us (44%)
  waiting for transfers between devices  123 us (27%)
  matrix products  41.5 us (9%)
  starting transfers between devices  31.4 us (7%)
  local copies, waits for them, and re-layouts  23.2 us (5%)
  other arithmetic  19.2 us (4%)
  between operations  14.6 us (3%)
    psum x2, blocking collectives, local(): lax.psum((jnp.sum(mixed, axis=-1), jnp.sum(mixed * mixed, axis=-1)), 'tp')  117 us
    reduce_scatter x2, waiting for transfers between devices, local(): lax.psum_scatter(partial_out, 'tp', scatter_dimension=2, tiled=True)  103 us
    all_gather x2, blocking collectives, local(): lax.all_gather(query_part, 'tp', axis=2, tiled=True)  47 us
    all_gather x2, blocking collectives, local(): lax.all_gather(key_part, 'tp', axis=2, tiled=True)  37.7 us
    ppermute x7, starting transfers between devices, collect(): lax.ppermute(going_down, axis, [(d, (d - 1) % ways) for d in range(ways)])  31.3 us
    ppermute x8, waiting for transfers between devices, collect(): lax.ppermute(going_up, axis, [(d, (d + 1) % ways) for d in range(ways)])  19.6 us
    dot_general x2, matrix products, local(): jnp.einsum('bthd,bhed->bthe', rot_q, state, precision=highest)  13.5 us
  transfers between devices with their start and end apart: 17, of which 10 were waited for; matrix products, arithmetic and copies ran while one was open for 3% of the time, Pallas kernels for 0%

profile of v1, /device:TPU:0, one launch (start us, length us, event | category | flops | bytes accessed | tf_op | source)
XLA Modules:
  0.0 454.2 jit_solution(17469151971419795445)
XLA Ops:
  7.3 0.7 bitcast_convert_fusion
  8.0 1.8 fusion.10
  9.9 0.8 slice_convert_fusion
  10.7 2.0 fusion.12
  13.0 1.8 convolution_convert_fusion.4
  15.3 24.6 %all_gather.12 = bf16[32,4,2048]{2,1,0:T(4,128)(2,1)S(1)} all-gather(bf16[32,4,128]{2,1,0:T(4,128)(2,1)S(1)} %bitcast.115), channel_id=1, replica_groups=mesh['grp'=2,'tp'=16] {'tp'}, dimensions={2}, use_global_device_ids=true | all-gather | bytes 557056 | tf_op jit(solution)/shard_map/all_gather | solution.py:106
  39.9 19.0 %all_gather.13 = bf16[32,4,2048]{2,1,0:T(4,128)(2,1)S(1)} all-gather(bf16[32,4,128]{2,1,0:T(4,128)(2,1)S(1)} %bitcast.114), channel_id=1, replica_groups=mesh['grp'=2,'tp'=16] {'tp'}, dimensions={2}, use_global_device_ids=true | all-gather | bytes 557056 | tf_op jit(solution)/shard_map/all_gather | solution.py:107
  59.4 0.6 multiply_subtract_fusion.2
  60.0 6.9 %fusion.4 = f32[32,8,4,16]{3,2,1,0:T(4,128)} fusion(f32[2,32,8,16,256]{4,3,2,1,0:T(8,128)} %param.10, f32[32,4,8,128]{3,1,2,0:T(4,128)S(1)} %get-tuple-element.48, f32[32,4,8,128]{3,1,2,0:T(4,128)S(1)} %get-tuple-element.49), kind=kOutput, calls=%fused_computation.7 | convolution fusion | flops 50593792 | bytes 5308416 | tf_op jit(solution)/shard_map/bthd,bhed->bthe/dot_general | solution.py:117
  66.9 2.0 copy.76
  69.0 2.7 fusion.56
  71.7 0.4 convolution_convert_fusion.6
  72.4 2.3 convolution_multiply_fusion.1
  74.8 1.0 fusion.38
  76.1 2.7 fusion.55
  79.7 1.8 fusion.54
  81.5 0.7 exponential_multiply_fusion
  82.4 59.1 %all-reduce.1 = (f32[32,4,8]{0,2,1:T(8,128)S(1)}, f32[32,4,8]{0,2,1:T(8,128)S(1)}) all-reduce(f32[32,4,8]{0,2,1:T(8,128)S(1)} %get-tuple-element.15, f32[32,4,8]{0,2,1:T(8,128)S(1)} %get-tuple-element.14), channel_id=1, replica_groups=mesh['grp'=2,'tp'=16] {'tp'}, use_global_device_ids=true, to_apply=%region_4.5 | all-reduce | flops 2048 | bytes 16384 | tf_op jit(solution)/shard_map/psum | solution.py:125
  141.7 1.8 fusion.57
  143.5 0.9 constant_dynamic-slice_fusion
  144.4 58.3 %reduce-scatter.3.cloned.1.call-done = f32[32,4,256]{2,0,1:T(8,128)} async-done(((f32[32,4,4096]{2,0,1:T(8,128)}), f32[32,4,256]{2,0,1:T(8,128)}) %reduce-scatter.3.cloned.1.call-update) | async-done | bytes 131088 | tf_op jit(solution)/shard_map/reduce_scatter | solution.py:139
  202.7 0.9 constant_dynamic-update-slice_fusion.15
  203.7 4.4 collective-permute-start.1
  208.2 1.9 collective-permute-done
  210.1 4.4 collective-permute-start.3
  214.6 2.0 collective-permute-done.2
  216.6 4.4 collective-permute-start.5
  221.1 1.9 collective-permute-done.4
  223.0 4.5 collective-permute-start.7
  227.5 1.9 collective-permute-done.6
  229.4 4.5 collective-permute-start.9
  233.9 1.9 collective-permute-done.8
  235.8 4.5 collective-permute-start.11
  240.3 1.9 collective-permute-done.10
  242.2 4.5 collective-permute-start.13
  246.7 1.9 collective-permute-done.12
  248.6 6.3 %collective-permute-done.14 = bf16[32,4,256]{2,0,1:T(8,128)(2,1)S(1)} collective-permute-done((bf16[32,4,256]{2,0,1:T(8,128)(2,1)S(1)}, bf16[32,4,256]{2,0,1:T(8,128)(2,1)S(1)}, u32[]{:S(2)}, u32[]{:S(2)}) %collective-permute-start.14) | collective-permute-done | bytes 65568 | tf_op jit(solution)/shard_map/ppermute | solution.py:19
  255.6 1.8 copy.78
  257.4 1.3 reshape.326
  258.7 1.7 convolution_convert_fusion
  260.5 1.7 convolution_convert_fusion.1
  263.3 18.7 %all_gather.15 = bf16[32,4,2048]{2,1,0:T(4,128)(2,1)S(1)} all-gather(bf16[32,4,128]{2,1,0:T(4,128)(2,1)S(1)} %bitcast.113), channel_id=1, replica_groups=mesh['grp'=2,'tp'=16] {'tp'}, dimensions={2}, use_global_device_ids=true | all-gather | bytes 557056 | tf_op jit(solution)/shard_map/all_gather | solution.py:107
  282.0 22.4 %all_gather.14 = bf16[32,4,2048]{2,1,0:T(4,128)(2,1)} all-gather(bf16[32,4,128]{2,1,0:T(4,128)(2,1)S(1)} %bitcast.112), channel_id=1, replica_groups=mesh['grp'=2,'tp'=16] {'tp'}, dimensions={2}, use_global_device_ids=true | all-gather | bytes 557056 | tf_op jit(solution)/shard_map/all_gather | solution.py:106
  304.4 1.0 reshape.346
  305.4 2.0 copy.80
  307.5 1.2 convert.12
  308.8 1.2 multiply_subtract_fusion
  310.0 0.8 copy-done.9
  311.0 6.6 %fusion = f32[32,8,4,16]{3,2,1,0:T(4,128)} fusion(f32[2,32,8,16,256]{4,3,2,1,0:T(8,128)} %param.10, f32[32,4,8,128]{3,1,2,0:T(4,128)S(1)} %get-tuple-element.46, f32[32,4,8,128]{3,1,2,0:T(4,128)S(1)} %get-tuple-element.47), kind=kOutput, calls=%fused_computation.2 | convolution fusion | flops 50593792 | bytes 5308416 | tf_op jit(solution)/shard_map/bthd,bhed->bthe/dot_general | solution.py:117
  317.6 1.3 copy.83
  318.9 3.7 convolution_multiply_fusion
  322.6 1.0 fusion.35
  323.6 1.0 copy.82
  324.6 1.1 fusion.50
  325.8 57.9 %all-reduce = (f32[32,4,8]{0,2,1:T(8,128)S(1)}, f32[32,4,8]{0,2,1:T(8,128)S(1)}) all-reduce(f32[32,4,8]{0,2,1:T(8,128)S(1)} %get-tuple-element.13, f32[32,4,8]{0,2,1:T(8,128)S(1)} %get-tuple-element.12), channel_id=1, replica_groups=mesh['grp'=2,'tp'=16] {'tp'}, use_global_device_ids=true, to_apply=%region_10.11 | all-reduce | flops 2048 | bytes 16384 | tf_op jit(solution)/shard_map/psum | solution.py:125
  383.7 1.1 multiply_convert_fusion
  384.8 1.8 fusion.58
  386.7 0.9 copy-done.5
  387.6 4.5 fusion.7
  392.2 4.5 fusion.3
  396.7 4.4 pad_maximum_fusion
  401.1 44.6 %reduce-scatter.5.cloned.1.call-done = f32[32,4,256]{2,0,1:T(8,128)} async-done(((f32[32,4,4096]{2,0,1:T(8,128)}), f32[32,4,256]{2,0,1:T(8,128)}) %reduce-scatter.5.cloned.1.call-update) | async-done | bytes 131088 | tf_op jit(solution)/shard_map/reduce_scatter | solution.py:139
  445.7 0.9 add_convert_fusion
  446.6 0.7 copy.88
  (96 shorter events, 5.8 us)
Async XLA Ops:
  7.2 195.5 %reduce-scatter.3.cloned.1.call-start = ((), (), s32[]{:S(2)}) async-start(), calls=%async_computation.2 | async-start | bytes 2228224 | tf_op jit(solution)/shard_map/reduce_scatter | solution.py:139
  13.0 1.9 copy-start.15
  60.0 12.4 %copy-start.2 = (f32[32,4,8,128]{3,1,2,0:T(4,128)}, f32[32,4,8,128]{3,1,2,0:T(4,128)S(1)}, u32[]{:S(2)}) copy-start(f32[32,4,8,128]{3,1,2,0:T(4,128)S(1)} %get-tuple-element.34) | copy-start | bytes 1572868
  60.0 12.4 %copy-start.4 = (f32[32,4,8,128]{3,1,2,0:T(4,128)}, f32[32,4,8,128]{3,1,2,0:T(4,128)S(1)}, u32[]{:S(2)}) copy-start(f32[32,4,8,128]{3,1,2,0:T(4,128)S(1)} %get-tuple-element.35) | copy-start | bytes 1572868
  72.4 2.3 copy-start.12
  79.7 2.5 copy-start.11
  143.5 302.3 %reduce-scatter.5.cloned.1.call-start = ((), (), s32[]{:S(2)}) async-start(), calls=%async_computation.3 | async-start | bytes 2228224 | tf_op jit(solution)/shard_map/reduce_scatter | solution.py:139
  203.7 6.4 %collective-permute-start = (bf16[32,4,256]{2,0,1:T(8,128)(2,1)S(1)}, bf16[32,4,256]{2,0,1:T(8,128)(2,1)S(1)}, u32[]{:S(2)}, u32[]{:S(2)}) collective-permute-start(bf16[32,4,256]{2,0,1:T(8,128)(2,1)S(1)} %get-tuple-element.22), channel_id=1, source_target_pairs={{0,1},{1,2},{2,3},{3,4},{4,5},{5,6},{6,7},{7,8},{8,9},{9,10},{10,1... | collective-permute-start | bytes 196616 | tf_op jit(solution)/shard_map/ppermute | solution.py:19
  203.7 6.4 %collective-permute-start.1 = (bf16[32,4,256]{2,0,1:T(8,128)(2,1)S(1)}, bf16[32,4,256]{2,0,1:T(8,128)(2,1)S(1)}, u32[]{:S(2)}, u32[]{:S(2)}) collective-permute-start(bf16[32,4,256]{2,0,1:T(8,128)(2,1)S(1)} %get-tuple-element.22), channel_id=1, source_target_pairs={{0,15},{1,0},{2,1},{3,2},{4,3},{5,4},{6,5},{7,6},{8,7},{9,8},{10,9... | collective-permute-start | bytes 196616 | tf_op jit(solution)/shard_map/ppermute | solution.py:22
  210.1 6.5 %collective-permute-start.2 = (bf16[32,4,256]{2,0,1:T(8,128)(2,1)S(1)}, bf16[32,4,256]{2,0,1:T(8,128)(2,1)S(1)}, u32[]{:S(2)}, u32[]{:S(2)}) collective-permute-start(bf16[32,4,256]{2,0,1:T(8,128)(2,1)S(1)} %collective-permute-done), channel_id=1, source_target_pairs={{0,1},{1,2},{2,3},{3,4},{4,5},{5,6},{6,7},{7,8},{8,9},{9,10},{10,1... | collective-permute-start | bytes 196616 | tf_op jit(solution)/shard_map/ppermute | solution.py:19
  210.1 6.5 %collective-permute-start.3 = (bf16[32,4,256]{2,0,1:T(8,128)(2,1)S(1)}, bf16[32,4,256]{2,0,1:T(8,128)(2,1)S(1)}, u32[]{:S(2)}, u32[]{:S(2)}) collective-permute-start(bf16[32,4,256]{2,0,1:T(8,128)(2,1)S(1)} %collective-permute-done.1), channel_id=1, source_target_pairs={{0,15},{1,0},{2,1},{3,2},{4,3},{5,4},{6,5},{7,6},{8,7},{9,8},{10,9... | collective-permute-start | bytes 196616 | tf_op jit(solution)/shard_map/ppermute | solution.py:22
  216.6 6.4 %collective-permute-start.4 = (bf16[32,4,256]{2,0,1:T(8,128)(2,1)S(1)}, bf16[32,4,256]{2,0,1:T(8,128)(2,1)S(1)}, u32[]{:S(2)}, u32[]{:S(2)}) collective-permute-start(bf16[32,4,256]{2,0,1:T(8,128)(2,1)S(1)} %collective-permute-done.2), channel_id=1, source_target_pairs={{0,1},{1,2},{2,3},{3,4},{4,5},{5,6},{6,7},{7,8},{8,9},{9,10},{10,1... | collective-permute-start | bytes 196616 | tf_op jit(solution)/shard_map/ppermute | solution.py:19
  216.6 6.4 %collective-permute-start.5 = (bf16[32,4,256]{2,0,1:T(8,128)(2,1)S(1)}, bf16[32,4,256]{2,0,1:T(8,128)(2,1)S(1)}, u32[]{:S(2)}, u32[]{:S(2)}) collective-permute-start(bf16[32,4,256]{2,0,1:T(8,128)(2,1)S(1)} %collective-permute-done.3), channel_id=1, source_target_pairs={{0,15},{1,0},{2,1},{3,2},{4,3},{5,4},{6,5},{7,6},{8,7},{9,8},{10,9... | collective-permute-start | bytes 196616 | tf_op jit(solution)/shard_map/ppermute | solution.py:22
  223.0 6.4 %collective-permute-start.6 = (bf16[32,4,256]{2,0,1:T(8,128)(2,1)S(1)}, bf16[32,4,256]{2,0,1:T(8,128)(2,1)S(1)}, u32[]{:S(2)}, u32[]{:S(2)}) collective-permute-start(bf16[32,4,256]{2,0,1:T(8,128)(2,1)S(1)} %collective-permute-done.4), channel_id=1, source_target_pairs={{0,1},{1,2},{2,3},{3,4},{4,5},{5,6},{6,7},{7,8},{8,9},{9,10},{10,1... | collective-permute-start | bytes 196616 | tf_op jit(solution)/shard_map/ppermute | solution.py:19
  223.0 6.4 %collective-permute-start.7 = (bf16[32,4,256]{2,0,1:T(8,128)(2,1)S(1)}, bf16[32,4,256]{2,0,1:T(8,128)(2,1)S(1)}, u32[]{:S(2)}, u32[]{:S(2)}) collective-permute-start(bf16[32,4,256]{2,0,1:T(8,128)(2,1)S(1)} %collective-permute-done.5), channel_id=1, source_target_pairs={{0,15},{1,0},{2,1},{3,2},{4,3},{5,4},{6,5},{7,6},{8,7},{9,8},{10,9... | collective-permute-start | bytes 196616 | tf_op jit(solution)/shard_map/ppermute | solution.py:22
  229.4 6.4 %collective-permute-start.8 = (bf16[32,4,256]{2,0,1:T(8,128)(2,1)S(1)}, bf16[32,4,256]{2,0,1:T(8,128)(2,1)S(1)}, u32[]{:S(2)}, u32[]{:S(2)}) collective-permute-start(bf16[32,4,256]{2,0,1:T(8,128)(2,1)S(1)} %collective-permute-done.6), channel_id=1, source_target_pairs={{0,1},{1,2},{2,3},{3,4},{4,5},{5,6},{6,7},{7,8},{8,9},{9,10},{10,1... | collective-permute-start | bytes 196616 | tf_op jit(solution)/shard_map/ppermute | solution.py:19
  229.4 6.4 %collective-permute-start.9 = (bf16[32,4,256]{2,0,1:T(8,128)(2,1)S(1)}, bf16[32,4,256]{2,0,1:T(8,128)(2,1)S(1)}, u32[]{:S(2)}, u32[]{:S(2)}) collective-permute-start(bf16[32,4,256]{2,0,1:T(8,128)(2,1)S(1)} %collective-permute-done.7), channel_id=1, source_target_pairs={{0,15},{1,0},{2,1},{3,2},{4,3},{5,4},{6,5},{7,6},{8,7},{9,8},{10,9... | collective-permute-start | bytes 196616 | tf_op jit(solution)/shard_map/ppermute | solution.py:22
  235.8 6.4 %collective-permute-start.10 = (bf16[32,4,256]{2,0,1:T(8,128)(2,1)S(1)}, bf16[32,4,256]{2,0,1:T(8,128)(2,1)S(1)}, u32[]{:S(2)}, u32[]{:S(2)}) collective-permute-start(bf16[32,4,256]{2,0,1:T(8,128)(2,1)S(1)} %collective-permute-done.8), channel_id=1, source_target_pairs={{0,1},{1,2},{2,3},{3,4},{4,5},{5,6},{6,7},{7,8},{8,9},{9,10},{10,1... | collective-permute-start | bytes 196616 | tf_op jit(solution)/shard_map/ppermute | solution.py:19
  235.8 6.4 %collective-permute-start.11 = (bf16[32,4,256]{2,0,1:T(8,128)(2,1)S(1)}, bf16[32,4,256]{2,0,1:T(8,128)(2,1)S(1)}, u32[]{:S(2)}, u32[]{:S(2)}) collective-permute-start(bf16[32,4,256]{2,0,1:T(8,128)(2,1)S(1)} %collective-permute-done.9), channel_id=1, source_target_pairs={{0,15},{1,0},{2,1},{3,2},{4,3},{5,4},{6,5},{7,6},{8,7},{9,8},{10,9... | collective-permute-start | bytes 196616 | tf_op jit(solution)/shard_map/ppermute | solution.py:22
  242.2 6.4 %collective-permute-start.12 = (bf16[32,4,256]{2,0,1:T(8,128)(2,1)S(1)}, bf16[32,4,256]{2,0,1:T(8,128)(2,1)S(1)}, u32[]{:S(2)}, u32[]{:S(2)}) collective-permute-start(bf16[32,4,256]{2,0,1:T(8,128)(2,1)S(1)} %collective-permute-done.10), channel_id=1, source_target_pairs={{0,1},{1,2},{2,3},{3,4},{4,5},{5,6},{6,7},{7,8},{8,9},{9,10},{10,1... | collective-permute-start | bytes 196616 | tf_op jit(solution)/shard_map/ppermute | solution.py:19
  242.2 6.4 %collective-permute-start.13 = (bf16[32,4,256]{2,0,1:T(8,128)(2,1)S(1)}, bf16[32,4,256]{2,0,1:T(8,128)(2,1)S(1)}, u32[]{:S(2)}, u32[]{:S(2)}) collective-permute-start(bf16[32,4,256]{2,0,1:T(8,128)(2,1)S(1)} %collective-permute-done.11), channel_id=1, source_target_pairs={{0,15},{1,0},{2,1},{3,2},{4,3},{5,4},{6,5},{7,6},{8,7},{9,8},{10,9... | collective-permute-start | bytes 196616 | tf_op jit(solution)/shard_map/ppermute | solution.py:22
  248.5 6.4 %collective-permute-start.14 = (bf16[32,4,256]{2,0,1:T(8,128)(2,1)S(1)}, bf16[32,4,256]{2,0,1:T(8,128)(2,1)S(1)}, u32[]{:S(2)}, u32[]{:S(2)}) collective-permute-start(bf16[32,4,256]{2,0,1:T(8,128)(2,1)S(1)} %collective-permute-done.12), channel_id=1, source_target_pairs={{0,1},{1,2},{2,3},{3,4},{4,5},{5,6},{6,7},{7,8},{8,9},{9,10},{10,1... | collective-permute-start | bytes 196616 | tf_op jit(solution)/shard_map/ppermute | solution.py:19
  258.7 3.5 copy-start
  260.5 2.2 copy-start.1
  310.0 0.8 copy-start.9
  310.0 1.0 copy-start.10
  310.0 8.9 %copy-start.6 = (f32[32,4,8,128]{3,1,2,0:T(4,128)}, f32[32,4,8,128]{3,1,2,0:T(4,128)S(1)}, u32[]{:S(2)}) copy-start(f32[32,4,8,128]{3,1,2,0:T(4,128)S(1)} %get-tuple-element.30) | copy-start | bytes 1572868
  311.0 7.9 %copy-start.13 = (f32[8,4,4]{2,1,0:T(4,128)S(1)}, f32[8,4,4]{2,1,0:T(4,128)}, u32[]{:S(2)}) copy-start(f32[8,4,4]{2,1,0:T(4,128)} %copy-done.12) | copy-start | bytes 1540
  384.8 1.8 copy-start.14
  384.8 1.9 copy-start.3
  386.6 1.0 copy-start.5
  387.6 4.5 copy-start.7
  387.6 4.5 copy-start.8
Sparse Core Ops, SparseCore 0:
  143.6 59.0 reduce-scatter.2
  386.7 58.9 reduce-scatter.4
